TPU v7x, 32 devices: a whole 2x2x4 slice. The times are simulated.
32 devices in a mesh: pp: 2 (over x), fs: 4 (over y, core), tp: 4 (over z).
Axes of the slice: x: 2, y: 2, z: 4, core: 2. Of those that a mesh axis runs over, the one named last changes fastest.
Arguments:
- inputs: bfloat16 [512, 2048], P('pp', ('fs', 'tp')), may hold values from -6 to 6
- norm_gain: bfloat16 [2, 2048], P('pp', ('fs', 'tp')), may hold values from 0.099609375 to 1.8984375
- w_value: bfloat16 [2, 2048, 2048], P('pp', None, ('fs', 'tp')), may hold values from -0.125 to 0.125
- w_gate: bfloat16 [2, 2048, 2048], P('pp', None, ('fs', 'tp')), may hold values from -0.125 to 0.125
- w_taps: bfloat16 [2, 31, 2048], P('pp', None, ('fs', 'tp')), may hold values from -1 to 1
- ln_gain: float32 [2, 2048], P('pp', ('fs', 'tp')), may hold values from 0.1 to 1.9
- ln_shift: float32 [2, 2048], P('pp', ('fs', 'tp')), may hold values from -3 to 3
Outputs:
- outputs: bfloat16 [512, 2048], P('pp', ('fs', 'tp'))
All inputs are finite; a program needn't handle non-finite values.
Results may differ from a plain program's by a relative error of at most 0.0085.
Values may be sent and summed in bfloat16 or wider, within the bound.
A program may use at most 64 MiB of HBM per device.

v0:
```python
import jax
import jax.numpy as jnp
from jax import lax
from jax.sharding import PartitionSpec as P

LEN = 128


norm_eps = 1e-06
layer_eps = 1e-05


def from_behind(block, axis, distance):
    devices = range(lax.axis_size(axis))
    route = [(i - distance, i) for i in devices if i - distance in devices]
    return lax.ppermute(block, axis, route)


def local(inputs, norm_gain, w_value, w_gate, w_taps, ln_gain, ln_shift):
    num_sections = lax.axis_size("pp")
    my_section = lax.axis_index("pp")
    model_width = w_value.shape[1]
    channels = w_value.shape[2]
    tap_count = w_taps.shape[1]
    fed_rows = lax.all_gather(inputs, "pp", axis=0, tiled=True)
    total_rows = fed_rows.shape[0]
    block_rows = LEN
    per_batch = LEN // block_rows
    block_count = total_rows // block_rows
    step_count = block_count + num_sections - 1
    gain_row = norm_gain[0]
    value_weight = w_value[0]
    gate_weight = w_gate[0]
    tap_weights = w_taps[0].astype(jnp.float32)
    layer_gain = ln_gain[0]
    layer_shift = ln_shift[0]

    def convolve(operands):
        history, gated_rows = operands
        padded = jnp.concatenate([history, gated_rows], axis=0)
        convolved = jnp.zeros((block_rows, channels), jnp.float32)
        for tap_index in range(tap_count):
            convolved = (
                convolved + padded[tap_index : tap_index + block_rows] * tap_weights[tap_index]
            )
        return convolved

    def skip_convolve(operands):
        return jnp.zeros((block_rows, channels), jnp.float32)

    def process_block(stream, history, active):
        stream_f = stream.astype(jnp.float32)
        zero_block = jnp.zeros((block_rows, channels), jnp.float32)
        squares = lax.psum(jnp.sum(stream_f * stream_f, axis=1), ("fs", "tp"))
        scale_rows = lax.rsqrt(squares / model_width + norm_eps)[:, None]
        normed = (stream_f * scale_rows * gain_row.astype(jnp.float32)).astype(jnp.bfloat16)
        shard_piece = lax.all_gather(normed, ("fs", "tp"), axis=1, tiled=True)

        def accumulate(current):
            return (
                jnp.dot(shard_piece, value_weight, preferred_element_type=jnp.float32),
                jnp.dot(shard_piece, gate_weight, preferred_element_type=jnp.float32),
            )

        def unchanged(current):
            return current

        value_sum, gate_sum = lax.cond(active, accumulate, unchanged, (zero_block, zero_block))
        gated_rows = value_sum * jax.nn.sigmoid(gate_sum)
        convolved = lax.cond(active, convolve, skip_convolve, (history, gated_rows))
        new_history = jnp.where(
            active, jnp.concatenate([history, gated_rows], axis=0)[block_rows:], history
        )
        moments = lax.psum(
            (jnp.sum(convolved, axis=1), jnp.sum(convolved * convolved, axis=1)), ("fs", "tp")
        )
        row_mean = moments[0][:, None] / model_width
        row_var = moments[1][:, None] / model_width - row_mean * row_mean
        normed_conv = (convolved - row_mean) * lax.rsqrt(
            row_var + layer_eps
        ) * layer_gain + layer_shift
        new_stream = (stream_f + jax.nn.silu(normed_conv)).astype(jnp.bfloat16)
        return (jnp.where(active, new_stream, stream), new_history)

    def step_body(step_index, loop_state):
        stream, history, results = loop_state
        block_index = step_index - my_section
        active = (block_index >= 0) & (block_index < block_count)
        safe_index = jnp.clip(block_index, 0, block_count - 1)
        row_offset = safe_index * block_rows
        first_rows = lax.dynamic_slice_in_dim(fed_rows, row_offset, block_rows, 0)
        stream = jnp.where(my_section == 0, first_rows, stream)
        history = jnp.where(
            active & (safe_index % per_batch == 0), jnp.zeros_like(history), history
        )
        new_stream, new_history = process_block(stream, history, active)
        previous = lax.dynamic_slice_in_dim(results, row_offset, block_rows, 0)
        keep_rows = active & (my_section == num_sections - 1)
        results = lax.dynamic_update_slice_in_dim(
            results, jnp.where(keep_rows, new_stream, previous), row_offset, 0
        )
        passed = from_behind(new_stream, "pp", 1)
        return (passed, new_history, results)

    initial = (
        jnp.zeros((block_rows, channels), jnp.bfloat16),
        jnp.zeros((tap_count - 1, channels), jnp.float32),
        jnp.zeros((total_rows, channels), jnp.bfloat16),
    )
    final_state = lax.fori_loop(0, step_count, step_body, initial)
    own_rows = inputs.shape[0]
    shares = final_state[2].reshape(num_sections, own_rows, channels)
    arrived = lax.all_to_all(shares, "pp", split_axis=0, concat_axis=0, tiled=True)
    return arrived[num_sections - 1]


def solution(mesh):
    in_specs = (
        P("pp", ("fs", "tp")),
        P("pp", ("fs", "tp")),
        P("pp", None, ("fs", "tp")),
        P("pp", None, ("fs", "tp")),
        P("pp", None, ("fs", "tp")),
        P("pp", ("fs", "tp")),
        P("pp", ("fs", "tp")),
    )
    out_specs = P("pp", ("fs", "tp"))
    return jax.shard_map(local, mesh=mesh, in_specs=in_specs, out_specs=out_specs, check_vma=False)
```

profile of v0, /device:TPU:3, one launch (start us, length us, event | category | flops | bytes accessed | tf_op | source)
XLA Modules:
  0.0 531.5 jit_solution(15302463253678728073)
XLA Ops:
  0.0 4.1 all_gather.13
  4.2 0.6 copy-done.1
  4.8 521.3 %while.20 = (s32[]{:T(128)}, bf16[128,128]{1,0:T(8,128)(2,1)S(1)}, f32[30,128]{1,0:T(8,128)S(1)}, bf16[512,128]{1,0:T(8,128)(2,1)S(1)}, s32[]{:T(128)}, /*index=...) while((s32[]{:T(128)}, bf16[128,128]{1,0:T(8,128)(2,1)S(1)}, ...), condition=%wide.region_11.12_spmd.clone, body=%wide.region_0.11_spmd.clone.sunk | while | flops 136179984 | bytes 5903558 | solution.py:110
  4.9 31.4 %psum.46 = f32[128]{0:T(128)S(1)} all-reduce(f32[128]{0:T(128)S(1)} %get-tuple-element.554), channel_id=1, replica_groups=mesh['pp'=2,'fs'=4,'tp'=4] {'fs','tp'}, use_global_device_ids=true, to_apply=%region_2.2 | all-reduce | flops 128 | bytes 1024 | tf_op jit(solution)/shard_map/while/body/eval_jaxpr/psum | solution.py:54
  36.4 32.3 %all_gather.16 = bf16[128,2048]{1,0:T(8,128)(2,1)S(1)} all-gather(bf16[128,128]{1,0:T(8,128)(2,1)S(1)} %fusion.106), channel_id=1, replica_groups=mesh['pp'=2,'fs'=4,'tp'=4] {'fs','tp'}, dimensions={1}, use_global_device_ids=true | all-gather | bytes 557056 | tf_op jit(solution)/shard_map/while/body/eval_jaxpr/all_gather | solution.py:57
  68.8 0.1 fusion.107
  68.9 32.0 %all-reduce.2 = (f32[128]{0:T(128)S(1)}, f32[128]{0:T(128)S(1)}) all-reduce(f32[128]{0:T(128)S(1)} %get-tuple-element.558, f32[128]{0:T(128)S(1)} %get-tuple-element.559), channel_id=1, replica_groups=mesh['pp'=2,'fs'=4,'tp'=4] {'fs','tp'}, use_global_device_ids=true, to_apply=%region_10.10 | all-reduce | flops 256 | bytes 2048 | tf_op jit(solution)/shard_map/while/body/eval_jaxpr/psum | solution.py:74
  100.9 0.1 select_dynamic-update-slice_fusion.2
  101.1 1.3 collective-permute-start
  102.4 3.4 collective-permute-done
  105.7 0.1 fusion.105
  105.8 31.3 %psum.46 = f32[128]{0:T(128)S(1)} all-reduce(f32[128]{0:T(128)S(1)} %get-tuple-element.554), channel_id=1, replica_groups=mesh['pp'=2,'fs'=4,'tp'=4] {'fs','tp'}, use_global_device_ids=true, to_apply=%region_2.2 | all-reduce | flops 128 | bytes 1024 | tf_op jit(solution)/shard_map/while/body/eval_jaxpr/psum | solution.py:54
  137.3 35.5 %all_gather.16 = bf16[128,2048]{1,0:T(8,128)(2,1)S(1)} all-gather(bf16[128,128]{1,0:T(8,128)(2,1)S(1)} %fusion.106), channel_id=1, replica_groups=mesh['pp'=2,'fs'=4,'tp'=4] {'fs','tp'}, dimensions={1}, use_global_device_ids=true | all-gather | bytes 557056 | tf_op jit(solution)/shard_map/while/body/eval_jaxpr/all_gather | solution.py:57
  172.8 1.6 conditional.6
  172.8 1.3 fusion
  174.1 0.3 fusion.97
  174.4 0.3 conditional.7
  174.5 0.2 fusion.5
  174.7 0.1 fusion.107
  174.8 30.6 %all-reduce.2 = (f32[128]{0:T(128)S(1)}, f32[128]{0:T(128)S(1)}) all-reduce(f32[128]{0:T(128)S(1)} %get-tuple-element.558, f32[128]{0:T(128)S(1)} %get-tuple-element.559), channel_id=1, replica_groups=mesh['pp'=2,'fs'=4,'tp'=4] {'fs','tp'}, use_global_device_ids=true, to_apply=%region_10.10 | all-reduce | flops 256 | bytes 2048 | tf_op jit(solution)/shard_map/while/body/eval_jaxpr/psum | solution.py:74
  205.4 0.1 select_dynamic-update-slice_fusion.2
  205.6 1.3 collective-permute-start
  206.9 3.4 collective-permute-done
  210.2 0.1 fusion.105
  210.4 33.2 %psum.46 = f32[128]{0:T(128)S(1)} all-reduce(f32[128]{0:T(128)S(1)} %get-tuple-element.554), channel_id=1, replica_groups=mesh['pp'=2,'fs'=4,'tp'=4] {'fs','tp'}, use_global_device_ids=true, to_apply=%region_2.2 | all-reduce | flops 128 | bytes 1024 | tf_op jit(solution)/shard_map/while/body/eval_jaxpr/psum | solution.py:54
  243.6 33.5 %all_gather.16 = bf16[128,2048]{1,0:T(8,128)(2,1)S(1)} all-gather(bf16[128,128]{1,0:T(8,128)(2,1)S(1)} %fusion.106), channel_id=1, replica_groups=mesh['pp'=2,'fs'=4,'tp'=4] {'fs','tp'}, dimensions={1}, use_global_device_ids=true | all-gather | bytes 557056 | tf_op jit(solution)/shard_map/while/body/eval_jaxpr/all_gather | solution.py:57
  277.2 1.6 conditional.6
  277.2 1.3 fusion
  278.5 0.3 fusion.97
  278.8 0.3 conditional.7
  278.9 0.2 fusion.5
  279.1 0.1 fusion.107
  279.3 31.9 %all-reduce.2 = (f32[128]{0:T(128)S(1)}, f32[128]{0:T(128)S(1)}) all-reduce(f32[128]{0:T(128)S(1)} %get-tuple-element.558, f32[128]{0:T(128)S(1)} %get-tuple-element.559), channel_id=1, replica_groups=mesh['pp'=2,'fs'=4,'tp'=4] {'fs','tp'}, use_global_device_ids=true, to_apply=%region_10.10 | all-reduce | flops 256 | bytes 2048 | tf_op jit(solution)/shard_map/while/body/eval_jaxpr/psum | solution.py:74
  311.2 0.1 select_dynamic-update-slice_fusion.2
  311.3 1.3 collective-permute-start
  312.6 3.4 collective-permute-done
  316.0 0.1 fusion.105
  316.1 31.0 %psum.46 = f32[128]{0:T(128)S(1)} all-reduce(f32[128]{0:T(128)S(1)} %get-tuple-element.554), channel_id=1, replica_groups=mesh['pp'=2,'fs'=4,'tp'=4] {'fs','tp'}, use_global_device_ids=true, to_apply=%region_2.2 | all-reduce | flops 128 | bytes 1024 | tf_op jit(solution)/shard_map/while/body/eval_jaxpr/psum | solution.py:54
  347.2 36.0 %all_gather.16 = bf16[128,2048]{1,0:T(8,128)(2,1)S(1)} all-gather(bf16[128,128]{1,0:T(8,128)(2,1)S(1)} %fusion.106), channel_id=1, replica_groups=mesh['pp'=2,'fs'=4,'tp'=4] {'fs','tp'}, dimensions={1}, use_global_device_ids=true | all-gather | bytes 557056 | tf_op jit(solution)/shard_map/while/body/eval_jaxpr/all_gather | solution.py:57
  383.2 1.6 conditional.6
  383.2 1.3 fusion
  384.5 0.3 fusion.97
  384.8 0.3 conditional.7
  384.9 0.2 fusion.5
  385.1 0.1 fusion.107
  385.2 30.6 %all-reduce.2 = (f32[128]{0:T(128)S(1)}, f32[128]{0:T(128)S(1)}) all-reduce(f32[128]{0:T(128)S(1)} %get-tuple-element.558, f32[128]{0:T(128)S(1)} %get-tuple-element.559), channel_id=1, replica_groups=mesh['pp'=2,'fs'=4,'tp'=4] {'fs','tp'}, use_global_device_ids=true, to_apply=%region_10.10 | all-reduce | flops 256 | bytes 2048 | tf_op jit(solution)/shard_map/while/body/eval_jaxpr/psum | solution.py:74
  415.8 0.1 select_dynamic-update-slice_fusion.2
  415.9 1.3 collective-permute-start
  417.2 3.4 collective-permute-done
  420.6 0.1 fusion.105
  420.7 33.2 %psum.46 = f32[128]{0:T(128)S(1)} all-reduce(f32[128]{0:T(128)S(1)} %get-tuple-element.554), channel_id=1, replica_groups=mesh['pp'=2,'fs'=4,'tp'=4] {'fs','tp'}, use_global_device_ids=true, to_apply=%region_2.2 | all-reduce | flops 128 | bytes 1024 | tf_op jit(solution)/shard_map/while/body/eval_jaxpr/psum | solution.py:54
  454.0 33.0 %all_gather.16 = bf16[128,2048]{1,0:T(8,128)(2,1)S(1)} all-gather(bf16[128,128]{1,0:T(8,128)(2,1)S(1)} %fusion.106), channel_id=1, replica_groups=mesh['pp'=2,'fs'=4,'tp'=4] {'fs','tp'}, dimensions={1}, use_global_device_ids=true | all-gather | bytes 557056 | tf_op jit(solution)/shard_map/while/body/eval_jaxpr/all_gather | solution.py:57
  487.0 1.6 conditional.6
  487.0 1.3 fusion
  488.4 0.3 fusion.97
  488.7 0.3 conditional.7
  488.8 0.2 fusion.5
  489.0 0.1 fusion.107
  489.1 32.3 %all-reduce.2 = (f32[128]{0:T(128)S(1)}, f32[128]{0:T(128)S(1)}) all-reduce(f32[128]{0:T(128)S(1)} %get-tuple-element.558, f32[128]{0:T(128)S(1)} %get-tuple-element.559), channel_id=1, replica_groups=mesh['pp'=2,'fs'=4,'tp'=4] {'fs','tp'}, use_global_device_ids=true, to_apply=%region_10.10 | all-reduce | flops 256 | bytes 2048 | tf_op jit(solution)/shard_map/while/body/eval_jaxpr/psum | solution.py:74
  521.4 0.1 select_dynamic-update-slice_fusion.2
  521.5 1.3 collective-permute-start
  522.8 3.4 collective-permute-done
  526.2 4.7 all_to_all.5
  530.9 0.6 slice_bitcast_fusion.31
  (65 shorter events, 1.0 us)
Async XLA Ops:
  0.0 4.1 copy-start.3
  4.1 0.7 copy-start.1
  4.2 0.7 copy-start.2
  4.2 0.7 copy-start.4
  4.8 63.9 %copy-start = (bf16[2048,128]{1,0:T(8,128)(2,1)S(1)}, bf16[2048,128]{1,0:T(8,128)(2,1)}, u32[]{:S(2)}) copy-start(bf16[2048,128]{1,0:T(8,128)(2,1)} %get-tuple-element.619) | copy-start | bytes 1572868 | tf_op jit(solution)/shard_map/while
  101.1 4.7 collective-permute-start
  105.7 67.0 %copy-start = (bf16[2048,128]{1,0:T(8,128)(2,1)S(1)}, bf16[2048,128]{1,0:T(8,128)(2,1)}, u32[]{:S(2)}) copy-start(bf16[2048,128]{1,0:T(8,128)(2,1)} %get-tuple-element.619) | copy-start | bytes 1572868 | tf_op jit(solution)/shard_map/while
  205.6 4.7 collective-permute-start
  210.2 66.9 %copy-start = (bf16[2048,128]{1,0:T(8,128)(2,1)S(1)}, bf16[2048,128]{1,0:T(8,128)(2,1)}, u32[]{:S(2)}) copy-start(bf16[2048,128]{1,0:T(8,128)(2,1)} %get-tuple-element.619) | copy-start | bytes 1572868 | tf_op jit(solution)/shard_map/while
  311.3 4.7 collective-permute-start
  316.0 67.2 %copy-start = (bf16[2048,128]{1,0:T(8,128)(2,1)S(1)}, bf16[2048,128]{1,0:T(8,128)(2,1)}, u32[]{:S(2)}) copy-start(bf16[2048,128]{1,0:T(8,128)(2,1)} %get-tuple-element.619) | copy-start | bytes 1572868 | tf_op jit(solution)/shard_map/while
  415.9 4.7 collective-permute-start
  420.6 66.4 %copy-start = (bf16[2048,128]{1,0:T(8,128)(2,1)S(1)}, bf16[2048,128]{1,0:T(8,128)(2,1)}, u32[]{:S(2)}) copy-start(bf16[2048,128]{1,0:T(8,128)(2,1)} %get-tuple-element.619) | copy-start | bytes 1572868 | tf_op jit(solution)/shard_map/while
  521.5 4.7 collective-permute-start
where the time goes:
time: 540 us; the launch traced here: 532 us
  blocking collectives  496 us (92%)
  waiting for transfers between devices  16.8 us (3%)
  starting transfers between devices  6.46 us (1%)
  matrix products  6.46 us (1%)
    all_gather x5, blocking collectives, process_block(): shard_piece = lax.all_gather(normed, ('fs', 'tp'), axis=1, tiled=True)  170 us
    psum x5, blocking collectives, process_block(): squares = lax.psum(jnp.sum(stream_f * stream_f, axis=1), ('fs', 'tp'))  160 us
    psum x5, blocking collectives, process_block(): lax.psum((jnp.sum(convolved, axis=1), jnp.sum(convolved * convolved, axis...  157 us
    ppermute x5, waiting for transfers between devices, from_behind(): return lax.ppermute(block, axis, route)  16.8 us
  transfers between devices with their start and end apart: 5, of which 5 were waited for; matrix products, arithmetic and copies ran while one was open for 0% of the time, Pallas kernels for 0%

commit v1 on v0

v1 whole, which is shorter than its diff:
```python
import functools

import jax
import jax.numpy as jnp
from jax import lax
from jax.experimental import pallas as pl
from jax.experimental.pallas import tpu as pltpu
from jax.sharding import PartitionSpec as P

LEN = 128


norm_eps = 1e-06
layer_eps = 1e-05
MESH = pl.DeviceIdType.MESH


def kernel(
    sizes,
    x_ref,
    gain_ref,
    wv_ref,
    wg_ref,
    taps_ref,
    lgain_ref,
    lshift_ref,
    out_ref,
    gath,
    gains,
    stat,
    hbuf,
    pad,
    taps,
    conv_buf,
    new_buf,
    turn,
    gath_sem,
    gain_sem,
    stat_sem,
    out_sem,
    feed_send,
    relay_send,
    gain_send,
    stat_send,
    next_send,
):
    P_, F, T = sizes
    G = F * T
    k, f, t = lax.axis_index("pp"), lax.axis_index("fs"), lax.axis_index("tp")
    M = gath.shape[0]
    C = x_ref.shape[1]
    D = wv_ref.shape[1]
    own_rows = x_ref.shape[0]
    piece = min(LEN, own_rows)
    per_mb = LEN // piece
    per_owner = own_rows // piece
    me = f * T + t
    ring_t = [lax.rem(t + d, T) for d in range(T)]
    pending = []

    def at(kk, ff, tt):
        return {"pp": kk, "fs": ff, "tp": tt}

    def send(src, dst, s_sem, r_sem, dev, cond=None):
        def make():
            return pltpu.make_async_remote_copy(
                src_ref=src, dst_ref=dst, send_sem=s_sem, recv_sem=r_sem,
                device_id=dev, device_id_type=MESH,
            )

        def go():
            make().start()

        def done():
            make().wait_send()

        if cond is None:
            go()
            pending.append(done)
        else:
            pl.when(cond)(go)
            pending.append(lambda: pl.when(cond)(done))

    def await_bytes(ref, sem):
        pltpu.make_async_copy(ref, ref, sem).wait()

    peers = []
    for df in range(F):
        for dt in range(T):
            if df or dt:
                peers.append(at(k, lax.rem(f + df, F), ring_t[dt]))
    others = []
    for dk in range(1, P_):
        for dt in range(T):
            others.append(at(lax.rem(k + dk, P_), f, ring_t[dt]))
    barrier = pltpu.get_barrier_semaphore()
    for dev in peers + others:
        pl.semaphore_signal(barrier, inc=1, device_id=dev, device_id_type=MESH)
    gains[me] = gain_ref[...].astype(jnp.float32)
    taps[...] = taps_ref[0].astype(jnp.float32)
    pad[0:32, :] = jnp.zeros((32, C), jnp.float32)
    turn[...] = jnp.zeros_like(turn)
    pl.semaphore_wait(barrier, len(peers) + len(others))

    for i in range(per_owner):
        p = k * per_owner + i
        m = lax.div(p, per_mb)
        rows = pl.ds(pl.multiple_of(lax.rem(p, per_mb) * piece, piece), piece)
        src = x_ref.at[pl.ds(i * piece, piece)]
        for dt in list(range(1, T)) + [0]:
            dst = gath.at[m, me, rows]
            sem = gath_sem.at[m, me]
            if dt == 0:
                @pl.when(k == 0)
                def _():
                    pltpu.make_async_copy(src, dst, sem).start()

                send(src, dst, feed_send.at[i, dt], sem, at(0, f, t), k != 0)
            else:
                send(src, dst, feed_send.at[i, dt], sem, at(0, f, ring_t[dt]))
        if i == 0:
            for n, dev in enumerate(peers):
                send(gains.at[me], gains.at[me], gain_send.at[n], gain_sem.at[0], dev)

    bits = []
    b = F // 2
    while b:
        bits.append(b)
        b //= 2

    def relay(m):
        count = 0
        for r in [0] + bits + [r for r in range(1, F) if r not in bits]:
            low = (r & -r) if r else F
            row = f ^ r
            for dt in range(T):
                slot = row * T + ring_t[dt]
                block = gath.at[m, slot]
                await_bytes(block, gath_sem.at[m, slot])
                for b in bits:
                    if b < low:
                        send(block, block, relay_send.at[m, count], gath_sem.at[m, slot], at(k, f ^ b, t))
                        count += 1

    def project(m):
        squares = jnp.zeros((LEN, C), jnp.float32)
        for s in range(G):
            xf = gath[m, s].astype(jnp.float32)
            squares = squares + xf * xf
            hbuf[:, s * C : (s + 1) * C] = (xf * gains[s]).astype(jnp.bfloat16)
        scale = lax.rsqrt(jnp.sum(squares, axis=1, keepdims=True) / D + norm_eps)
        value = jnp.dot(hbuf[...], wv_ref[0], preferred_element_type=jnp.float32) * scale
        gate = jnp.dot(hbuf[...], wg_ref[0], preferred_element_type=jnp.float32) * scale
        pad[32:, :] = value * jax.nn.sigmoid(gate)
        W = taps.shape[0]
        step = 32
        for r0 in range(0, LEN, step):
            acc = jnp.zeros((step, C), jnp.float32)
            for j in range(W):
                o = 32 - (W - 1) + j + r0
                acc = acc + pad[o : o + step, :] * taps[j : j + 1, :]
            conv_buf[m, r0 : r0 + step, :] = acc
        conv = conv_buf[m]
        lane = lax.broadcasted_iota(jnp.int32, (LEN, LEN), 1)
        s1 = jnp.sum(conv, axis=1, keepdims=True)
        s2 = jnp.sum(conv * conv, axis=1, keepdims=True)
        both = jnp.where(lane == 0, s1, jnp.where(lane == 1, s2, 0.0))
        stat[m, me] = both.T[0:2, :]
        for n, dev in enumerate(peers):
            send(stat.at[m, me], stat.at[m, me], stat_send.at[m, n], stat_sem.at[m], dev)

    def finish(m):
        await_bytes(stat.at[m, pl.ds(0, G - 1)], stat_sem.at[m])
        turn[0:2, :] = jnp.sum(stat[m], axis=0)
        cols = turn[...].T
        mu = cols[:, 0:1] / D
        var = cols[:, 1:2] / D - mu * mu
        y = (conv_buf[m] - mu) * lax.rsqrt(var + layer_eps) * lgain_ref[...] + lshift_ref[...]
        new = (gath[m, me].astype(jnp.float32) + y * jax.nn.sigmoid(y)).astype(jnp.bfloat16)
        new_buf[m] = new
        for dt in list(range(1, T)) + [0]:
            if P_ > 1:
                send(
                    new_buf.at[m], gath.at[m, me], next_send.at[m, dt], gath_sem.at[m, me],
                    at(lax.rem(k + 1, P_), f, ring_t[dt]), k < P_ - 1,
                )
        for q in range(per_mb):
            p = m * per_mb + q
            owner, i = p // per_owner, p % per_owner
            rows = pl.ds(i * piece, piece)
            part = pl.ds(q * piece, piece)
            if owner == P_ - 1:
                @pl.when(k == P_ - 1)
                def _():
                    out_ref[rows, :] = new_buf[m, part, :]
            else:
                send(
                    new_buf.at[m, part], out_ref.at[rows], next_send.at[m, q], out_sem.at[i],
                    at(owner, f, t), k == P_ - 1,
                )

    for m in range(M):
        relay(m)
        if m == 0:
            await_bytes(gains.at[pl.ds(0, G - 1)], gain_sem.at[0])
        project(m)
        if m:
            finish(m - 1)
    finish(M - 1)
    if P_ > 1:
        @pl.when(k < P_ - 1)
        def _():
            for i in range(per_owner):
                await_bytes(out_ref.at[pl.ds(i * piece, piece)], out_sem.at[i])
    for done in pending:
        done()


def local(sizes, inputs, norm_gain, w_value, w_gate, w_taps, ln_gain, ln_shift):
    P_, F, T = sizes
    G = F * T
    own_rows, C = inputs.shape
    M = own_rows * P_ // LEN
    piece = min(LEN, own_rows)
    per_owner = own_rows // piece
    per_mb = LEN // piece
    D = w_value.shape[1]
    W = w_taps.shape[1]
    bits = F.bit_length() - 1
    relays = T * (F - 1) if bits else 1
    dma = pltpu.SemaphoreType.DMA
    f32, bf16 = jnp.float32, jnp.bfloat16
    return pl.pallas_call(
        functools.partial(kernel, sizes),
        out_shape=jax.ShapeDtypeStruct((own_rows, C), bf16),
        in_specs=[pl.BlockSpec(memory_space=pltpu.VMEM)] * 7,
        out_specs=pl.BlockSpec(memory_space=pltpu.VMEM),
        scratch_shapes=[
            pltpu.VMEM((M, G, LEN, C), bf16),
            pltpu.VMEM((G, 1, C), f32),
            pltpu.VMEM((M, G, 2, LEN), f32),
            pltpu.VMEM((LEN, D), bf16),
            pltpu.VMEM((LEN + 32, C), f32),
            pltpu.VMEM((W, C), f32),
            pltpu.VMEM((M, LEN, C), f32),
            pltpu.VMEM((M, LEN, C), bf16),
            pltpu.VMEM((LEN, LEN), f32),
            dma((M, G)),
            dma((1,)),
            dma((M,)),
            dma((per_owner,)),
            dma((per_owner, T)),
            dma((M, relays)),
            dma((G - 1,)),
            dma((M, G - 1)),
            dma((M, max(T, per_mb))),
        ],
        compiler_params=pltpu.CompilerParams(collective_id=0, has_side_effects=True),
    )(inputs, norm_gain, w_value, w_gate, w_taps, ln_gain, ln_shift)


def solution(mesh):
    sizes = (mesh.shape["pp"], mesh.shape["fs"], mesh.shape["tp"])
    in_specs = (
        P("pp", ("fs", "tp")),
        P("pp", ("fs", "tp")),
        P("pp", None, ("fs", "tp")),
        P("pp", None, ("fs", "tp")),
        P("pp", None, ("fs", "tp")),
        P("pp", ("fs", "tp")),
        P("pp", ("fs", "tp")),
    )
    out_specs = P("pp", ("fs", "tp"))
    return jax.shard_map(
        functools.partial(local, sizes), mesh=mesh, in_specs=in_specs, out_specs=out_specs,
        check_vma=False,
    )
```

time: 540 us -> 62.9 us (0.12); the launches traced: 532 us -> 62.7 us
  blocking collectives: 496 us -> 0 us
  Pallas kernels: 0 us -> 61.2 us
  waiting for transfers between devices: 16.8 us -> 0 us
  matrix products: 6.46 us -> 0 us
  starting transfers between devices: 6.46 us -> 0 us
    psum x10 -> x0, blocking collectives: 317 us -> none  [the longest x5 160 us: process_block(): squares = lax.psum(jnp.sum(stream_f * stream_f, axis=1), ('fs', 'tp'))]
    all_gather x6 -> x0, blocking collectives: 174 us -> none  [the longest x5 170 us: process_block(): shard_piece = lax.all_gather(normed, ('fs', 'tp'), axis=1, tiled=True)]
    pallas_call x0 -> x1, Pallas kernels: none -> 61.2 us  [local(): pl.pallas_call(functools.partial(kernel, sizes), out_shape=jax.ShapeDtype...]
    ppermute x5 -> x0, waiting for transfers between devices: 16.8 us -> none  [from_behind(): return lax.ppermute(block, axis, route)]
    dot_general x8 -> x0, matrix products: 6.46 us -> none  [the longest x4 5.32 us: accumulate(): jnp.dot(shard_piece, gate_weight, preferred_element_type=jnp.float32)]
    ppermute x5 -> x0, starting transfers between devices: 6.46 us -> none  [from_behind(): return lax.ppermute(block, axis, route)]
  transfers between devices with their start and end apart: 5 -> 0, of which waited for: 5 -> 0; matrix products, arithmetic and copies ran while one was open for 0% -> 0% of each run, Pallas kernels for 0% -> 0%
where the time goes in v1:
time: 62.9 us; the launch traced here: 62.7 us
  Pallas kernels  61.2 us (97%)
  local copies, waits for them, and re-layouts  1.47 us (2%)
    pallas_call x1, Pallas kernels, local(): pl.pallas_call(functools.partial(kernel, sizes), out_shape=jax.ShapeDtype...  61.2 us
    unnamed x1, local copies, waits for them, and re-layouts  1.47 us

profile of v1, /device:TPU:3, one launch (start us, length us, event | category | flops | bytes accessed | tf_op | source)
XLA Modules:
  0.0 62.7 jit_solution(655465522386609884)
XLA Ops:
  0.0 61.2 %shard_map.73 = bf16[256,128]{1,0:T(8,128)(2,1)} custom-call(bf16[256,128]{1,0:T(8,128)(2,1)} %x_ref.1, bf16[1,128]{1,0:T(2,128)(2,1)} %gain_ref.1, bf16[1,2048,128]{2,1,0:T(8,128)(2,1)} %wv_ref.1, bf16[1,2048,128]{2,1,0:T(8,128)(2,1)} %wg_ref.1, bf16[1,31,128]{2,1,0:T(8,128)(2,1)} %taps_ref.1, f32[1,128]{1,0:T(1,128)} %lgain_ref.1, f32[1,128]{1,0:T(1,128)} %lshift_ref.1), custom_call_target="tpu_custom_call" | custom-call | tf_op jit(solution)/shard_map/pallas_call | solution.py:233
  61.3 1.5 %copy.9 = bf16[256,128]{1,0:T(8,128)(2,1)} copy(bf16[256,128]{1,0:T(8,128)(2,1)} %shard_map.73) | data formatting | bytes 131072

commit v2 on v1

v2 whole, which is shorter than its diff:
```python
import functools

import jax
import jax.numpy as jnp
from jax import lax
from jax.experimental import pallas as pl
from jax.experimental.pallas import tpu as pltpu
from jax.sharding import PartitionSpec as P

LEN = 128


norm_eps = 1e-06
layer_eps = 1e-05
MESH = pl.DeviceIdType.MESH


def kernel(
    sizes,
    x_hbm,
    gain_hbm,
    wv_hbm,
    wg_hbm,
    taps_hbm,
    lgain_hbm,
    lshift_hbm,
    out_ref,
    x_ref,
    gain_ref,
    wv_ref,
    wg_ref,
    taps_ref,
    lgain_ref,
    lshift_ref,
    load_sem,
    gath,
    gains,
    stat,
    hbuf,
    pad,
    taps,
    conv_buf,
    new_buf,
    turn,
    gath_sem,
    gain_sem,
    stat_sem,
    out_sem,
    feed_send,
    relay_send,
    gain_send,
    stat_send,
    next_send,
    back_send,
):
    P_, F, T = sizes
    G = F * T
    k, f, t = lax.axis_index("pp"), lax.axis_index("fs"), lax.axis_index("tp")
    M = gath.shape[0]
    C = x_ref.shape[1]
    D = wv_ref.shape[1]
    own_rows = x_ref.shape[0]
    piece = min(LEN, own_rows)
    per_mb = LEN // piece
    per_owner = own_rows // piece
    head = pad.shape[0] - LEN
    me = f * T + t
    loads = [
        pltpu.make_async_copy(a, b, load_sem.at[n])
        for n, (a, b) in enumerate(
            [
                (x_hbm, x_ref), (gain_hbm, gain_ref), (wv_hbm, wv_ref), (wg_hbm, wg_ref),
                (taps_hbm, taps_ref), (lgain_hbm, lgain_ref), (lshift_hbm, lshift_ref),
            ]
        )
    ]
    for load in loads:
        load.start()
    if T & (T - 1) == 0:
        to_t = [t] + [t ^ d for d in range(T - 1, 0, -1)]
        from_t = to_t
    else:
        to_t = [lax.rem(t + d, T) for d in range(T)]
        from_t = [lax.rem(t + T - d, T) for d in range(T)]

    def at(kk, ff, tt):
        return {"pp": kk, "fs": ff, "tp": tt}

    def send(src, dst, s_sem, r_sem, dev, cond=None):
        def go():
            pltpu.make_async_remote_copy(
                src_ref=src, dst_ref=dst, send_sem=s_sem, recv_sem=r_sem,
                device_id=dev, device_id_type=MESH,
            ).start()

        if cond is None:
            go()
        else:
            pl.when(cond)(go)

    def await_bytes(ref, sem):
        pltpu.make_async_copy(ref, ref, sem).wait()

    peers = []
    for dt in list(range(1, T)) + [0]:
        for df in range(F):
            if df or dt:
                peers.append(at(k, lax.rem(f + df, F), to_t[dt]))
    others = []
    for dk in range(1, P_):
        for dt in range(T):
            others.append(at(lax.rem(k + dk, P_), f, to_t[dt]))
    barrier = pltpu.get_barrier_semaphore()
    for dev in peers + others:
        pl.semaphore_signal(barrier, inc=1, device_id=dev, device_id_type=MESH)
    for load in loads[:2]:
        load.wait()
    gains[me] = gain_ref[...].astype(jnp.float32)
    pad[0:head, :] = jnp.zeros((head, C), jnp.float32)
    turn[...] = jnp.zeros_like(turn)
    pl.semaphore_wait(barrier, len(peers) + len(others))

    for i in range(per_owner):
        p = k * per_owner + i
        m = lax.div(p, per_mb)
        rows = pl.ds(pl.multiple_of(lax.rem(p, per_mb) * piece, piece), piece)
        src = x_ref.at[pl.ds(i * piece, piece)]
        dst = gath.at[m, me, rows]
        sem = gath_sem.at[m, me]

        @pl.when(k == 0)
        def _():
            pltpu.make_async_copy(src, dst, sem).start()

        send(src, dst, feed_send.at[0], sem, at(0, f, t), k != 0)
        for dt in range(1, T):
            send(src, dst, feed_send.at[1], sem, at(0, f, to_t[dt]))
        if i == 0:
            for dev in peers:
                send(gains.at[me], gains.at[me], gain_send.at[0], gain_sem.at[0], dev)
    for load in loads[2:]:
        load.wait()
    taps[...] = taps_ref[0].astype(jnp.float32)

    bits = []
    b = F // 2
    while b:
        bits.append(b)
        b //= 2

    def relay(m, low):
        for r in range(F):
            if ((r & -r) if r else F) == low:
                for tt in from_t:
                    slot = (f ^ r) * T + tt
                    block = gath.at[m, slot]
                    await_bytes(block, gath_sem.at[m, slot])
                    for b in bits:
                        if b < low:
                            send(block, block, relay_send.at[0], gath_sem.at[m, slot], at(k, f ^ b, t))

    def project(m):
        squares = jnp.zeros((LEN, C), jnp.float32)
        for s in range(G):
            xf = gath[m, s].astype(jnp.float32)
            squares = squares + xf * xf
            hbuf[:, s * C : (s + 1) * C] = (xf * gains[s]).astype(jnp.bfloat16)
        scale = lax.rsqrt(jnp.sum(squares, axis=1, keepdims=True) / D + norm_eps)
        value = jnp.dot(hbuf[...], wv_ref[0], preferred_element_type=jnp.float32) * scale
        gate = jnp.dot(hbuf[...], wg_ref[0], preferred_element_type=jnp.float32) * scale
        pad[head:, :] = value * jax.nn.sigmoid(gate)
        W = taps.shape[0]
        step = 32
        for r0 in range(0, LEN, step):
            acc = jnp.zeros((step, C), jnp.float32)
            for j in range(W):
                o = head - (W - 1) + j + r0
                acc = acc + pad[o : o + step, :] * taps[j : j + 1, :]
            conv_buf[m, r0 : r0 + step, :] = acc
        conv = conv_buf[m]
        lane = lax.broadcasted_iota(jnp.int32, (LEN, LEN), 1)
        s1 = jnp.sum(conv, axis=1, keepdims=True)
        s2 = jnp.sum(conv * conv, axis=1, keepdims=True)
        both = jnp.where(lane == 0, s1, jnp.where(lane == 1, s2, 0.0))
        stat[m, me] = both.T[0:2, :]
        for dev in peers:
            send(stat.at[m, me], stat.at[m, me], stat_send.at[0], stat_sem.at[m], dev)

    def finish(m):
        await_bytes(stat.at[m, pl.ds(0, G - 1)], stat_sem.at[m])
        turn[0:2, :] = jnp.sum(stat[m], axis=0)
        cols = turn[...].T
        mu = cols[:, 0:1] / D
        var = cols[:, 1:2] / D - mu * mu
        y = (conv_buf[m] - mu) * lax.rsqrt(var + layer_eps) * lgain_ref[...] + lshift_ref[...]
        new = (gath[m, me].astype(jnp.float32) + y * jax.nn.sigmoid(y)).astype(jnp.bfloat16)
        new_buf[m] = new
        if P_ > 1:
            for tt in to_t:
                send(
                    new_buf.at[m], gath.at[m, me], next_send.at[0], gath_sem.at[m, me],
                    at(lax.rem(k + 1, P_), f, tt), k < P_ - 1,
                )
        for q in range(per_mb):
            p = m * per_mb + q
            owner, i = p // per_owner, p % per_owner
            rows = pl.ds(i * piece, piece)
            part = pl.ds(q * piece, piece)
            if owner == P_ - 1:
                @pl.when(k == P_ - 1)
                def _():
                    out_ref[rows, :] = new_buf[m, part, :]
            else:
                send(
                    new_buf.at[m, part], out_ref.at[rows], back_send.at[0], out_sem.at[i],
                    at(owner, f, t), k == P_ - 1,
                )

    levels = [F] + bits
    relay(0, F)
    for m in range(M):
        if m + 1 < M:
            relay(m + 1, F)
        for low in levels[1:]:
            relay(m, low)
        if m == 0:
            await_bytes(gains.at[pl.ds(0, G - 1)], gain_sem.at[0])
        project(m)
        if m:
            finish(m - 1)
    await_bytes(gath.at[:, pl.ds(0, T * (F - 1))], relay_send.at[0])
    await_bytes(stat.at[:, pl.ds(0, G - 1)], stat_send.at[0])
    await_bytes(gains.at[pl.ds(0, G - 1)], gain_send.at[0])
    for i in range(per_owner):
        await_bytes(gath.at[0, pl.ds(0, T - 1), pl.ds(0, piece)], feed_send.at[1])
    if P_ > 1:
        @pl.when(k != 0)
        def _():
            await_bytes(x_ref, feed_send.at[0])

    finish(M - 1)
    if P_ > 1:
        @pl.when(k < P_ - 1)
        def _():
            await_bytes(gath.at[:, pl.ds(0, T)], next_send.at[0])
            for i in range(per_owner):
                await_bytes(out_ref.at[pl.ds(i * piece, piece)], out_sem.at[i])

        @pl.when(k == P_ - 1)
        def _():
            for _i in range(per_owner * (P_ - 1)):
                await_bytes(out_ref.at[pl.ds(0, piece)], back_send.at[0])


def local(sizes, inputs, norm_gain, w_value, w_gate, w_taps, ln_gain, ln_shift):
    P_, F, T = sizes
    G = F * T
    own_rows, C = inputs.shape
    M = own_rows * P_ // LEN
    piece = min(LEN, own_rows)
    per_owner = own_rows // piece
    per_mb = LEN // piece
    D = w_value.shape[1]
    W = w_taps.shape[1]
    head = -(-(W - 1) // 8) * 8
    operands = (inputs, norm_gain, w_value, w_gate, w_taps, ln_gain, ln_shift)
    dma = pltpu.SemaphoreType.DMA
    f32, bf16 = jnp.float32, jnp.bfloat16
    return pl.pallas_call(
        functools.partial(kernel, sizes),
        out_shape=jax.ShapeDtypeStruct((own_rows, C), bf16),
        in_specs=[pl.BlockSpec(memory_space=pl.ANY)] * 7,
        out_specs=pl.BlockSpec(memory_space=pltpu.VMEM),
        scratch_shapes=[
            *[pltpu.VMEM(a.shape, a.dtype) for a in operands],
            dma((len(operands),)),
            pltpu.VMEM((M, G, LEN, C), bf16),
            pltpu.VMEM((G, 1, C), f32),
            pltpu.VMEM((M, G, 2, LEN), f32),
            pltpu.VMEM((LEN, D), bf16),
            pltpu.VMEM((LEN + head, C), f32),
            pltpu.VMEM((W, C), f32),
            pltpu.VMEM((M, LEN, C), f32),
            pltpu.VMEM((M, LEN, C), bf16),
            pltpu.VMEM((LEN, LEN), f32),
            dma((M, G)),
            dma((1,)),
            dma((M,)),
            dma((per_owner,)),
            dma((2,)),
            dma((1,)),
            dma((1,)),
            dma((1,)),
            dma((1,)),
            dma((1,)),
        ],
        compiler_params=pltpu.CompilerParams(collective_id=0, has_side_effects=True),
    )(*operands)


def solution(mesh):
    sizes = (mesh.shape["pp"], mesh.shape["fs"], mesh.shape["tp"])
    in_specs = (
        P("pp", ("fs", "tp")),
        P("pp", ("fs", "tp")),
        P("pp", None, ("fs", "tp")),
        P("pp", None, ("fs", "tp")),
        P("pp", None, ("fs", "tp")),
        P("pp", ("fs", "tp")),
        P("pp", ("fs", "tp")),
    )
    out_specs = P("pp", ("fs", "tp"))
    return jax.shard_map(
        functools.partial(local, sizes), mesh=mesh, in_specs=in_specs, out_specs=out_specs,
        check_vma=False,
    )
```

time: 62.9 us -> 48.7 us (0.77)
  Pallas kernels: 61.2 us -> 47.1 us
    pallas_call x1, Pallas kernels: 61.2 us -> 47.1 us  [local(): pl.pallas_call(functools.partial(kernel, sizes), out_shape=jax.ShapeDtype...]
where the time goes in v2:
time: 48.7 us; the launch traced here: 48.6 us
  Pallas kernels  47.1 us (97%)
  local copies, waits for them, and re-layouts  1.47 us (3%)
    pallas_call x1, Pallas kernels, local(): pl.pallas_call(functools.partial(kernel, sizes), out_shape=jax.ShapeDtype...  47.1 us
    unnamed x1, local copies, waits for them, and re-layouts  1.47 us

profile of v2, /device:TPU:3, one launch (start us, length us, event | category | flops | bytes accessed | tf_op | source)
XLA Modules:
  0.0 48.6 jit_solution(418859369957195504)
XLA Ops:
  0.0 47.1 %shard_map.73 = bf16[256,128]{1,0:T(8,128)(2,1)} custom-call(bf16[256,128]{1,0:T(8,128)(2,1)} %x_hbm.1, bf16[1,128]{1,0:T(2,128)(2,1)} %gain_hbm.1, bf16[1,2048,128]{2,1,0:T(8,128)(2,1)} %wv_hbm.1, bf16[1,2048,128]{2,1,0:T(8,128)(2,1)} %wg_hbm.1, bf16[1,31,128]{2,1,0:T(8,128)(2,1)} %taps_hbm.1, f32[1,128]{1,0:T(1,128)} %lgain_hbm.1, f32[1,128]{1,0:T(1,128)} %lshift_hbm.1), custom_call_target="tpu_custom_call" | custom-call | tf_op jit(solution)/shard_map/pallas_call | solution.py:269
  47.1 1.5 %copy.9 = bf16[256,128]{1,0:T(8,128)(2,1)} copy(bf16[256,128]{1,0:T(8,128)(2,1)} %shard_map.73) | data formatting | bytes 131072

commit v3 on v2

--- a/solution.py
+++ b/solution.py
@@ -217,17 +217,34 @@
                 )
 
     levels = [F] + bits
-    relay(0, F)
-    for m in range(M):
-        if m + 1 < M:
-            relay(m + 1, F)
-        for low in levels[1:]:
-            relay(m, low)
-        if m == 0:
-            await_bytes(gains.at[pl.ds(0, G - 1)], gain_sem.at[0])
-        project(m)
-        if m:
-            finish(m - 1)
+
+    def run(ahead, lag):
+        for m in range(min(ahead, M)):
+            relay(m, F)
+        for m in range(M):
+            if ahead == 1 and m + 1 < M:
+                relay(m + 1, F)
+            for low in levels[1:-1]:
+                relay(m, low)
+            if ahead > 1 and m + ahead < M:
+                relay(m + ahead, F)
+            if lag > 1 and m > 1:
+                finish(m - 2)
+            if len(levels) > 1:
+                relay(m, levels[-1])
+            if m == 0:
+                await_bytes(gains.at[pl.ds(0, G - 1)], gain_sem.at[0])
+            project(m)
+            if lag == 1 and m:
+                finish(m - 1)
+        if lag > 1 and M > 1:
+            finish(M - 2)
+
+    if P_ == 1:
+        run(2, 1)
+    else:
+        pl.when(k == 0)(lambda: run(1, 1))
+        pl.when(k != 0)(lambda: run(1, 2))
     await_bytes(gath.at[:, pl.ds(0, T * (F - 1))], relay_send.at[0])
     await_bytes(stat.at[:, pl.ds(0, G - 1)], stat_send.at[0])
     await_bytes(gains.at[pl.ds(0, G - 1)], gain_send.at[0])

time: 48.7 us -> 48.5 us (level)
  no operation moved by 1% of the time
where the time goes in v3:
time: 48.5 us; the launch traced here: 48.3 us
  Pallas kernels  46.8 us (96%)
  local copies, waits for them, and re-layouts  1.47 us (3%)
    pallas_call x1, Pallas kernels, local(): pl.pallas_call(functools.partial(kernel, sizes), out_shape=jax.ShapeDtype...  46.8 us
    unnamed x1, local copies, waits for them, and re-layouts  1.47 us

profile of v3, /device:TPU:3, one launch (start us, length us, event | category | flops | bytes accessed | tf_op | source)
XLA Modules:
  0.0 48.3 jit_solution(18305948279456401567)
XLA Ops:
  0.0 46.8 %shard_map.73 = bf16[256,128]{1,0:T(8,128)(2,1)} custom-call(bf16[256,128]{1,0:T(8,128)(2,1)} %x_hbm.1, bf16[1,128]{1,0:T(2,128)(2,1)} %gain_hbm.1, bf16[1,2048,128]{2,1,0:T(8,128)(2,1)} %wv_hbm.1, bf16[1,2048,128]{2,1,0:T(8,128)(2,1)} %wg_hbm.1, bf16[1,31,128]{2,1,0:T(8,128)(2,1)} %taps_hbm.1, f32[1,128]{1,0:T(1,128)} %lgain_hbm.1, f32[1,128]{1,0:T(1,128)} %lshift_hbm.1), custom_call_target="tpu_custom_call" | custom-call | tf_op jit(solution)/shard_map/pallas_call | solution.py:286
  46.8 1.5 %copy.9 = bf16[256,128]{1,0:T(8,128)(2,1)} copy(bf16[256,128]{1,0:T(8,128)(2,1)} %shard_map.73) | data formatting | bytes 131072
